TPU v7x, 32 devices: a whole 2x2x4 slice. The times are simulated.
32 devices in a mesh: sp: 16 (over z, y, x), tp: 2 (over core).
Axes of the slice: x: 2, y: 2, z: 4, core: 2. Of those that a mesh axis runs over, the one named last changes fastest.
Arguments:
- tokens: bfloat16 [2048, 2048], P(('sp', 'tp')), may hold values from -6 to 6
- input_norm_gain: float32 [2048], replicated, may hold values from 0.1 to 1.9
- differential_query: bfloat16 [2048, 1024], P(None, 'tp'), may hold values from -0.176776695 to 0.176776695, as said below
- differential_key: bfloat16 [2048, 1024], P(None, 'tp'), may hold values from -0.176776695 to 0.176776695, as said below
- differential_value: bfloat16 [2048, 1024], P(None, 'tp'), may hold values from -0.125 to 0.125
- query_norm_gain: float32 [64], replicated, may hold values from 1.15 to 5
- key_norm_gain: float32 [64], replicated, may hold values from 1.15 to 5
- second_map_weight: float32 [8], P('tp'), may hold values from 0.3 to 0.8
- differential_norm_gain: float32 [128], replicated, may hold values from 0.1 to 1.9
- linear_query: bfloat16 [2048, 512], P(None, 'tp'), may hold values from -0.125 to 0.125
- linear_key: bfloat16 [2048, 512], P(None, 'tp'), may hold values from -0.125 to 0.125
- linear_value: bfloat16 [2048, 1024], P(None, 'tp'), may hold values from -0.125 to 0.125
- linear_output_gate: bfloat16 [2048, 1024], P(None, 'tp'), may hold values from -0.125 to 0.125
- forget_down_factor: bfloat16 [2048, 32], replicated, may hold values from -0.125 to 0.125
- forget_up_factor: bfloat16 [32, 512], P(None, 'tp'), may hold values from -2.109375 to 2.109375
- forget_bias: float32 [512], P('tp'), may hold values from -0.5 to 10
- extra_shrinkage_exponent: float32 [2048, 8], P('sp', 'tp'), may hold values from -1.5 to 0
- linear_norm_gain: float32 [128], replicated, may hold values from 0.1 to 1.9
- differential_output_rows: bfloat16 [1024, 2048], P('tp'), may hold values from -0.125 to 0.125
- linear_output_rows: bfloat16 [1024, 2048], P('tp'), may hold values from -0.125 to 0.125
Outputs:
- layer_out: bfloat16 [2048, 2048], P(('sp', 'tp'))
Inputs may be any that keep to these rules, and one draw needn't show every extreme that they name: `differential_query`: independent entries of scale one over sqrt(2048). `differential_key`: entries of scale one over sqrt(2048).
All inputs are finite; a program needn't handle non-finite values.
Results may differ from a plain program's by a relative error of at most 0.015.
Values may be sent and summed in bfloat16 or wider, within the bound.
A program may use at most 64 MiB of HBM per device.

v0:
```python
from functools import partial
import jax
import jax.numpy as jnp
from jax import lax
from jax.sharding import PartitionSpec as P

HEAD = 64
VDIM = 128
RECURRENT_DIM = 64
GLA_DV = 128
BLOCK = 64
RMS_EPS = 1e-06
SOFTMAX_DIVISOR = 16.0
OUT_SCALE = 0.8
NEG_LARGE = -1e30
HIGHEST = lax.Precision.HIGHEST


def partner(block, axis, apart):
    count = lax.axis_size(axis)
    route = []
    for low in range(count):
        high = low | 1 << apart
        if high != low and high < count:
            route += [(low, high), (high, low)]
    return lax.ppermute(block, axis, route)


def prefix(shard, axis, combine, identity):
    devices, position = (lax.axis_size(axis), lax.axis_index(axis))
    everything = jax.tree.map(lambda part: lax.all_gather(part, axis), shard)
    start = jax.tree.map(
        lambda part, zero: jnp.broadcast_to(jnp.asarray(zero, part.dtype), part.shape),
        shard,
        identity,
    )

    def turn(k, before):
        reached = k < position
        new = combine(before, jax.tree.map(lambda part: part[k], everything))
        return jax.tree.map(lambda a, b: jnp.where(reached, a, b), new, before)

    return lax.fori_loop(0, devices, turn, start)


def rms_scale(values, scale_gain):
    mean_sq = jnp.mean(values * values, axis=-1, keepdims=True)
    return values * lax.rsqrt(mean_sq + RMS_EPS) * scale_gain


def block_length(total_rows, shard_rows):
    best = shard_rows
    shard_total = total_rows // shard_rows
    for multiple in range(1, shard_total + 1):
        if shard_total % multiple == 0 and shard_rows * multiple <= 2048:
            best = shard_rows * multiple
    return best


def combine_chain(earlier, later):
    return (earlier[0] * later[0], earlier[1] * later[0][..., None] + later[1])


def keep_carry(carry_now):
    return carry_now


def attend_span(query_set, query_pos, keys_here, values_here, key_pos, carry_now):
    row_peaks, totals, numerators = carry_now
    query_rows = query_set.shape[0]
    group_count = query_set.shape[1]
    attn_heads = group_count // 2
    span_rows = keys_here.shape[0]
    scores = jnp.einsum(
        "tgd,kgd->gtk", query_set, keys_here, preferred_element_type=jnp.float32
    ) * HEAD ** (-0.5)
    causal = key_pos[None, :] <= query_pos[:, None]
    scores = jnp.where(causal[None], scores, NEG_LARGE)
    new_peaks = jnp.maximum(row_peaks, jnp.max(scores, axis=-1))
    weights = jnp.where(causal[None], jnp.exp(scores - new_peaks[..., None]), 0.0)
    factor = jnp.exp(row_peaks - new_peaks)
    totals = totals * factor + jnp.sum(weights, axis=-1)
    rounded = weights.astype(jnp.bfloat16).reshape(attn_heads, 2, query_rows, span_rows)
    contrib = jnp.einsum(
        "hmtk,khv->hmtv", rounded, values_here, preferred_element_type=jnp.float32
    ).reshape(group_count, query_rows, VDIM)
    return (new_peaks, totals, numerators * factor[..., None] + contrib)


def per_device(
    tokens,
    input_norm_gain,
    differential_query,
    differential_key,
    differential_value,
    query_norm_gain,
    key_norm_gain,
    second_map_weight,
    differential_norm_gain,
    linear_query,
    linear_key,
    linear_value,
    linear_output_gate,
    forget_down_factor,
    forget_up_factor,
    forget_bias,
    extra_shrinkage_exponent,
    linear_norm_gain,
    differential_output_rows,
    linear_output_rows,
):
    sp_size = lax.axis_size("sp")
    sp_index = lax.axis_index("sp")
    attn_heads = second_map_weight.shape[0]
    linear_head_list = extra_shrinkage_exponent.shape[1]
    normed = rms_scale(tokens.astype(jnp.float32), input_norm_gain).astype(jnp.bfloat16)
    parts_list = [
        differential_query,
        differential_key,
        differential_value,
        linear_query,
        linear_key,
        linear_value,
        linear_output_gate,
        forget_down_factor,
    ]
    packed = jnp.concatenate(parts_list, axis=1)
    bounds = [0]
    for matrix in parts_list:
        bounds.append(bounds[-1] + matrix.shape[1])
    projected = jnp.dot(
        lax.all_gather(normed, "tp", axis=0, tiled=True), packed, preferred_element_type=jnp.float32
    ).astype(jnp.bfloat16)
    row_count = projected.shape[0]
    half_rows = row_count // 2
    bit_count = sp_size.bit_length() - 1

    def section(column_set):
        return projected[:, bounds[column_set] : bounds[column_set + 1]]

    group_count = 2 * attn_heads
    query_norm = rms_scale(
        section(0).astype(jnp.float32).reshape(row_count, group_count, HEAD), query_norm_gain
    ).astype(jnp.bfloat16)
    key_norm = rms_scale(
        section(1).astype(jnp.float32).reshape(row_count, group_count, HEAD), key_norm_gain
    ).astype(jnp.bfloat16)
    key_flat = key_norm.reshape(row_count, group_count * HEAD)
    value_flat = section(2)
    far_queries = query_norm[half_rows:].reshape(half_rows, group_count * HEAD)
    for bit in range(bit_count):
        far_queries = partner(far_queries, "sp", bit)
    mirror_index = sp_size - 1 - sp_index
    own_pos = sp_index * row_count + jnp.arange(half_rows, dtype=jnp.int32)
    far_pos = mirror_index * row_count + half_rows + jnp.arange(half_rows, dtype=jnp.int32)
    query_sets = [
        (query_norm[:half_rows], own_pos),
        (far_queries.reshape(half_rows, group_count, HEAD), far_pos),
    ]
    fold_start = tuple(
        (
            (
                jnp.full((group_count, query_set.shape[0]), NEG_LARGE, jnp.float32),
                jnp.zeros((group_count, query_set.shape[0]), jnp.float32),
                jnp.zeros((group_count, query_set.shape[0], VDIM), jnp.float32),
            )
            for query_set, query_pos in query_sets
        )
    )
    key_rows = lax.all_gather(key_flat, "sp", axis=0, tiled=True)
    value_rows = lax.all_gather(value_flat, "sp", axis=0, tiled=True)
    piece_rows = key_rows.shape[0]
    span_rows = block_length(piece_rows, row_count)

    def attend(span_index, carries):
        row_start = span_index * span_rows
        keys_here = lax.dynamic_slice_in_dim(
            key_rows, span_index * span_rows, span_rows, 0
        ).reshape(span_rows, group_count, HEAD)
        values_here = lax.dynamic_slice_in_dim(
            value_rows, span_index * span_rows, span_rows, 0
        ).reshape(span_rows, attn_heads, VDIM)
        key_pos = row_start + jnp.arange(span_rows, dtype=jnp.int32)
        results = []
        for (query_set, query_pos), carry_in in zip(query_sets, carries):
            work = partial(attend_span, query_set, query_pos, keys_here, values_here, key_pos)
            results.append(lax.cond(row_start <= jnp.max(query_pos), work, keep_carry, carry_in))
        return tuple(results)

    folded = lax.fori_loop(0, piece_rows // span_rows, attend, fold_start)

    def finish(carry_set):
        row_peaks, totals, numerators = carry_set
        set_rows = totals.shape[1]
        maps_out = (numerators / totals[..., None]).reshape(attn_heads, 2, set_rows, VDIM)
        attn_mix = maps_out[:, 0] - second_map_weight[:, None, None] * maps_out[:, 1]
        return (
            (rms_scale(attn_mix, differential_norm_gain) * OUT_SCALE)
            .transpose(1, 0, 2)
            .reshape(set_rows, attn_heads * VDIM)
            .astype(jnp.bfloat16)
        )

    own_rows = finish(folded[0])
    far_rows = finish(folded[1])
    for bit in range(bit_count):
        far_rows = partner(far_rows, "sp", bit)
    attn_out = jnp.concatenate([own_rows, far_rows], axis=0)
    chain_queries = section(3).astype(jnp.float32).reshape(
        row_count, linear_head_list, RECURRENT_DIM
    ) * RECURRENT_DIM ** (-0.5)
    chain_keys = section(4).astype(jnp.float32).reshape(row_count, linear_head_list, RECURRENT_DIM)
    chain_values = section(5).astype(jnp.float32).reshape(row_count, linear_head_list, GLA_DV)
    gated = jax.nn.silu(section(6).astype(jnp.float32)).reshape(row_count, linear_head_list, GLA_DV)
    sigmoid_preactivation = (
        jnp.dot(section(7), forget_up_factor, preferred_element_type=jnp.float32) + forget_bias
    )
    shrinkage_exponent = (
        jax.nn.log_sigmoid(sigmoid_preactivation).reshape(
            row_count, linear_head_list, RECURRENT_DIM
        )
        / SOFTMAX_DIVISOR
        + extra_shrinkage_exponent[:, :, None]
    )
    block_total = row_count // BLOCK

    def blockify(array):
        return array.reshape(block_total, BLOCK, linear_head_list, array.shape[-1])

    causal_block = jnp.arange(BLOCK)[:, None] >= jnp.arange(BLOCK)[None, :]

    def chain_block(carry, inputs):
        carried, log_total = carry
        query_block, key_block, value_block, decay_block = inputs
        log_cum = jnp.cumsum(decay_block, axis=0)
        log_last = log_cum[-1]
        query_decayed = query_block * jnp.exp(log_cum)
        key_inverse = key_block * jnp.exp(-log_cum)
        inner_scores = jnp.einsum("thd,shd->hts", query_decayed, key_inverse, precision=HIGHEST)
        inner_scores = jnp.where(causal_block[None], inner_scores, 0.0)
        local_out = jnp.einsum("hts,she->the", inner_scores, value_block, precision=HIGHEST)
        local_out = local_out + jnp.einsum(
            "thd,hde->the", query_decayed, carried, precision=HIGHEST
        )
        key_end = key_block * jnp.exp(log_last[None] - log_cum)
        carried = carried * jnp.exp(log_last)[..., None] + jnp.einsum(
            "thd,the->hde", key_end, value_block, precision=HIGHEST
        )
        carried_query = query_decayed * jnp.exp(log_total)[None]
        return ((carried, log_total + log_last), (local_out, carried_query))

    chain_zero = (
        jnp.zeros((linear_head_list, RECURRENT_DIM, GLA_DV), jnp.float32),
        jnp.zeros((linear_head_list, RECURRENT_DIM), jnp.float32),
    )
    (own_state, log_total), (local_out, carried_query) = lax.scan(
        chain_block,
        chain_zero,
        (
            blockify(chain_queries),
            blockify(chain_keys),
            blockify(chain_values),
            blockify(shrinkage_exponent),
        ),
    )
    local_out = local_out.reshape(row_count, linear_head_list, GLA_DV)
    carried_query = carried_query.reshape(row_count, linear_head_list, RECURRENT_DIM)
    own_decay = jnp.exp(log_total)
    carried_in = prefix(
        (own_decay, own_state),
        "sp",
        combine_chain,
        (jnp.ones_like(own_decay), jnp.zeros_like(own_state)),
    )[1]
    chain_full = local_out + jnp.einsum(
        "thd,hde->the", carried_query, carried_in, precision=HIGHEST
    )
    chain_out = (
        (rms_scale(chain_full, linear_norm_gain) * gated)
        .reshape(row_count, linear_head_list * GLA_DV)
        .astype(jnp.bfloat16)
    )
    return lax.psum_scatter(
        (
            jnp.dot(attn_out, differential_output_rows, preferred_element_type=jnp.float32)
            + jnp.dot(chain_out, linear_output_rows, preferred_element_type=jnp.float32)
        ).astype(jnp.bfloat16),
        "tp",
        scatter_dimension=0,
        tiled=True,
    )


def solution(mesh):
    placed = (
        P(("sp", "tp"), None),
        P(),
        P(None, "tp"),
        P(None, "tp"),
        P(None, "tp"),
        P(),
        P(),
        P("tp"),
        P(),
        P(None, "tp"),
        P(None, "tp"),
        P(None, "tp"),
        P(None, "tp"),
        P(),
        P(None, "tp"),
        P("tp"),
        P("sp", "tp"),
        P(),
        P("tp", None),
        P("tp", None),
    )
    return jax.shard_map(
        per_device, mesh=mesh, in_specs=placed, out_specs=P(("sp", "tp"), None), check_vma=False
    )
```

profile of v0, /device:TPU:0, one launch (start us, length us, event | category | flops | bytes accessed | tf_op | source)
XLA Modules:
  0.0 273.5 jit_solution(2683229393621899004)
XLA Ops:
  6.6 3.3 %constant_dynamic-update-slice_fusion.7 = bf16[2048,3104]{1,0:T(8,128)(2,1)} fusion(bf16[2048,512]{1,0:T(8,128)(2,1)} %param.30), kind=kLoop, calls=%fused_computation.130 | loop fusion | bytes 4194304
  10.5 2.4 all_gather.21
  13.0 3.2 %constant_dynamic-update-slice_fusion.6 = bf16[2048,3104]{1,0:T(8,128)(2,1)} fusion(bf16[2048,3104]{1,0:T(8,128)(2,1)} %constant_dynamic-update-slice_fusion.7, bf16[2048,512]{1,0:T(8,128)(2,1)} %param.31), kind=kLoop, calls=%fused_computation.129 | loop fusion | bytes 4194304
  16.2 1.5 constant_dynamic-update-slice_fusion.5
  17.8 1.1 constant_dynamic-update-slice_fusion.4
  18.8 1.1 constant_dynamic-update-slice_fusion.3
  19.9 1.6 constant_dynamic-update-slice_fusion.2
  21.5 1.5 constant_dynamic-update-slice_fusion.1
  23.9 8.3 %convolution_convert_fusion = bf16[128,3104]{0,1:T(8,128)(2,1)S(1)} fusion(bf16[128,2048]{1,0:T(8,128)(2,1)S(1)} %all_gather.21, bf16[2048,3104]{1,0:T(8,128)(2,1)} %constant_dynamic-update-slice_fusion), kind=kOutput, calls=%fused_computation.68 | convolution fusion | flops 1627787264 | bytes 14032896 | tf_op jit(solution)/shard_map/dot_general | solution.py:131
  35.4 1.1 reshape.228
  36.5 1.2 copy.125
  38.7 1.1 div.64
  39.9 1.1 mul.296
  41.0 1.8 reshape.219
  43.7 10.5 %while.8 = (s32[]{:T(128)}, f32[4,64,128]{2,1,0:T(8,128)S(1)}, f32[4,64]{1,0:T(4,128)S(1)}, f32[2,64,4,128]{3,1,0,2:T(8,128)}, f32[2,64,4,64]{3,2,1,0:T(4,128)},...) while((s32[]{:T(128)}, f32[4,64,128]{2,1,0:T(8,128)S(1)}, ...), condition=%wide.region_17.18_spmd.clone, body=%wide.region_15.0_spmd.clone.sunk | while | flops 89412096 | bytes 2970753 | solution.py:256
  43.7 1.2 constant_dynamic-slice_fusion.3
  49.0 1.2 constant_dynamic-slice_fusion.3
  55.6 2.9 %collective-permute-start = (bf16[64,512]{1,0:T(8,128)(2,1)S(1)}, bf16[64,512]{1,0:T(8,128)(2,1)S(1)}, u32[]{:S(2)}, u32[]{:S(2)}) collective-permute-start(bf16[64,512]{1,0:T(8,128)(2,1)S(1)} %reshape.212), channel_id=1, source_target_pairs={{0,2},{2,0},{4,6},{6,4},{8,10},{10,8},{12,14},{14,12},{16,18},{18,... | collective-permute-start | bytes 196616 | tf_op jit(solution)/shard_map/ppermute | solution.py:26
  58.5 2.4 collective-permute-done
  60.9 1.9 collective-permute-start.1
  64.7 1.1 copy.129
  65.8 40.7 %all-gather.2 = f32[16,4,64]{2,1,0:T(4,128)S(1)} all-gather(f32[1,4,64]{2,1,0:T(4,128)S(1)} %exponential_bitcast_fusion), channel_id=2, replica_groups=mesh['sp'=16,'tp'=2] {'sp'}, dimensions={0}, use_global_device_ids=true | all-gather | bytes 17408 | tf_op jit(solution)/shard_map/all_gather | solution.py:31
  106.6 4.3 %collective-permute-done.2 = bf16[64,512]{1,0:T(8,128)(2,1)S(1)} collective-permute-done((bf16[64,512]{1,0:T(8,128)(2,1)S(1)}, bf16[64,512]{1,0:T(8,128)(2,1)S(1)}, u32[]{:S(2)}, u32[]{:S(2)}) %collective-permute-start.2) | collective-permute-done | bytes 65568 | tf_op jit(solution)/shard_map/ppermute | solution.py:26
  110.9 52.9 %all-gather.9.cloned.1.call-done = bf16[2048,512]{0,1:T(8,128)(2,1)} async-done(((bf16[128,512]{0,1:T(8,128)(2,1)}), bf16[2048,512]{0,1:T(8,128)(2,1)}) %all-gather.9.cloned.1.call-update) | async-done | bytes 2097168 | tf_op jit(solution)/shard_map/all_gather | solution.py:171
  163.8 5.5 %conditional.3 = (f32[8,64]{1,0:T(8,128)S(1)}, f32[8,64,128]{2,1,0:T(8,128)S(1)}) conditional(s32[]{:T(128)} %convert_element_type.81, (f32[8,64]{1,0:T(8,128)S(1)}, f32[8,64,128]{2,1,0:T(8,128)S(1)}) %tuple.49, (s32[2048]{0:T(1024)S(1)}, s32[64]{0:T(128)S(1)}, bf16[64,512]{1,0:T(8,128)(2,1)S(1)}, bf16[2048,8,64]{0,2,1:T(8,128)(2,1)}, ...), branch_computations={%region_10.0_spmd, %region_11.0_spmd} | conditional | flops 412353536 | bytes 26839340 | solution.py:187
  164.3 2.6 fusion.9
  166.9 1.3 fusion.10
  169.4 5.3 %conditional.2 = ((f32[8,64]{1,0:T(8,128)S(1)}, f32[8,64,128]{2,1,0:T(8,128)S(1)})) conditional(s32[]{:T(128)} %convert_element_type.71, (f32[8,64]{1,0:T(8,128)S(1)}, f32[8,64,128]{2,1,0:T(8,128)S(1)}) %tuple.49, (s32[2048]{0:T(1024)S(1)}, s32[64]{0:T(128)S(1)}, bf16[128,8,64]{2,0,1:T(8,128)(2,1)S(1)}, bf16[2048,8,64]{0,2,1:T(8,128)(2,1)}, ...), branch_computations={%region_4.5_spmd, %region_5.8_spmd} | conditional | flops 412353536 | bytes 26773812 | solution.py:187
  169.6 2.6 fusion.2
  172.2 1.3 fusion.3
  176.0 1.5 collective-permute-start.4
  177.4 47.9 %all-gather.11.cloned.1.call-done = f32[64,64,128]{2,1,0:T(8,128)} async-done(((f32[4,64,128]{2,1,0:T(8,128)}), f32[64,64,128]{2,1,0:T(8,128)}) %all-gather.11.cloned.1.call-update) | async-done | bytes 2097168 | tf_op jit(solution)/shard_map/all_gather | solution.py:31
  225.4 17.2 %while.9 = (s32[]{:T(128)}, f32[4,64,128]{2,1,0:T(8,128)S(1)}, s32[]{:T(128)}, f32[16,4,64]{2,1,0:T(4,128)S(1)}, f32[16,4,64,128]{3,2,1,0:T(8,128)}, /*index=5*/s32[]{:T(128)}, s32[]{:T(128)}) while((s32[]{:T(128)}, f32[4,64,128]{2,1,0:T(8,128)S(1)}, s32[]{:T(128)}, f32[16,4,64]{2,1,0:T(4,128)S(1)}, ...), condition=%wide.region_19.20_spmd.clone, body=%wide.region_18.19_spmd.clone.sunk | while | flops 131076 | bytes 396393 | solution.py:43
  226.5 1.0 fusion.107
  227.5 1.0 fusion.107
  228.6 1.0 fusion.107
  229.7 1.0 fusion.107
  230.8 1.0 fusion.107
  231.9 1.0 fusion.107
  242.7 1.7 multiply_reduce_fusion
  244.4 1.5 collective-permute-start.5
  245.9 2.8 %collective-permute-done.5 = bf16[64,512]{1,0:T(8,128)(2,1)S(1)} collective-permute-done((bf16[64,512]{1,0:T(8,128)(2,1)S(1)}, bf16[64,512]{1,0:T(8,128)(2,1)S(1)}, u32[]{:S(2)}, u32[]{:S(2)}) %collective-permute-start.5) | collective-permute-done | bytes 65568 | tf_op jit(solution)/shard_map/ppermute | solution.py:26
  248.7 1.5 collective-permute-start.6
  250.3 2.7 collective-permute-done.6
  253.0 1.8 collective-permute-start.7
  255.3 2.9 %collective-permute-done.7 = bf16[64,512]{1,0:T(8,128)(2,1)S(1)} collective-permute-done((bf16[64,512]{1,0:T(8,128)(2,1)S(1)}, bf16[64,512]{1,0:T(8,128)(2,1)S(1)}, u32[]{:S(2)}, u32[]{:S(2)}) %collective-permute-start.7) | collective-permute-done | bytes 65568 | tf_op jit(solution)/shard_map/ppermute | solution.py:26
  258.2 1.3 fusion.41
  259.4 7.6 %reduce-scatter.2.cloned.1.call-done = bf16[64,2048]{1,0:T(8,128)(2,1)} async-done(((bf16[128,2048]{1,0:T(8,128)(2,1)}), bf16[64,2048]{1,0:T(8,128)(2,1)}) %reduce-scatter.2.cloned.1.call-update) | async-done | bytes 262160 | tf_op jit(solution)/shard_map/reduce_scatter | solution.py:283
  (168 shorter events, 31.6 us)
Async XLA Ops:
  6.5 248.2 %copy-start = (bf16[512,2048]{1,0:T(8,128)(2,1)S(1)}, bf16[512,2048]{1,0:T(8,128)(2,1)}, u32[]{:S(2)}) copy-start(bf16[512,2048]{1,0:T(8,128)(2,1)} %param.47) | copy-start | bytes 6291460
  6.5 3.4 %copy-start.12 = (bf16[2048,32]{0,1:T(8,128)(2,1)S(1)}, bf16[2048,32]{0,1:T(8,128)(2,1)}, u32[]{:S(2)}) copy-start(bf16[2048,32]{0,1:T(8,128)(2,1)} %param.41) | copy-start | bytes 393220
  6.5 3.7 %copy-start.8 = (bf16[64,2048]{1,0:T(8,128)(2,1)S(1)}, bf16[64,2048]{1,0:T(8,128)(2,1)}, u32[]{:S(2)}) copy-start(bf16[64,2048]{1,0:T(8,128)(2,1)} %param.28) | copy-start | bytes 786436
  6.5 3.9 %copy-start.13 = (f32[2048]{0:T(1024)S(1)}, f32[2048]{0:T(1024)}, u32[]{:S(2)}) copy-start(f32[2048]{0:T(1024)} %param.29) | copy-start | bytes 24580
  6.5 104.3 %all-gather.7.cloned.1.call-start = ((), (), s32[]{:S(2)}) async-start(), calls=%async_computation.1 | async-start | bytes 2228224 | tf_op jit(solution)/shard_map/all_gather | solution.py:170
  10.2 6.0 %copy-start.4 = (bf16[2048,512]{1,0:T(8,128)(2,1)S(1)}, bf16[2048,512]{1,0:T(8,128)(2,1)}, u32[]{:S(2)}) copy-start(bf16[2048,512]{1,0:T(8,128)(2,1)} %param.32) | copy-start | bytes 6291460
  13.0 4.8 %copy-start.9 = (bf16[2048,256]{1,0:T(8,128)(2,1)S(1)}, bf16[2048,256]{1,0:T(8,128)(2,1)}, u32[]{:S(2)}) copy-start(bf16[2048,256]{1,0:T(8,128)(2,1)} %param.37) | copy-start | bytes 3145732
  16.2 2.6 copy-start.10
  16.2 3.7 %copy-start.5 = (bf16[2048,512]{1,0:T(8,128)(2,1)S(1)}, bf16[2048,512]{1,0:T(8,128)(2,1)}, u32[]{:S(2)}) copy-start(bf16[2048,512]{1,0:T(8,128)(2,1)} %param.39) | copy-start | bytes 6291460
  17.8 3.8 %copy-start.6 = (bf16[2048,512]{1,0:T(8,128)(2,1)S(1)}, bf16[2048,512]{1,0:T(8,128)(2,1)}, u32[]{:S(2)}) copy-start(bf16[2048,512]{1,0:T(8,128)(2,1)} %param.40) | copy-start | bytes 6291460
  23.9 8.4 %copy-start.16 = (f32[64]{0:T(128)S(1)}, f32[64]{0:T(128)}, u32[]{:S(2)}) copy-start(f32[64]{0:T(128)} %param.34) | copy-start | bytes 772
  23.9 13.8 %copy-start.20 = (bf16[32,256]{1,0:T(8,128)(2,1)S(1)}, bf16[32,256]{1,0:T(8,128)(2,1)}, u32[]{:S(2)}) copy-start(bf16[32,256]{1,0:T(8,128)(2,1)} %param.42) | copy-start | bytes 49156
  23.9 13.9 %copy-start.21 = (f32[256]{0:T(256)S(1)}, f32[256]{0:T(256)}, u32[]{:S(2)}) copy-start(f32[256]{0:T(256)} %param.43) | copy-start | bytes 3076
  32.2 7.6 %copy-start.14 = (f32[128,4]{0,1:T(4,128)S(1)}, f32[128,4]{0,1:T(4,128)}, u32[]{:S(2)}) copy-start(f32[128,4]{0,1:T(4,128)} %param.44) | copy-start | bytes 6148
  33.3 130.5 %all-gather.9.cloned.1.call-start = ((), (), s32[]{:S(2)}) async-start(), calls=%async_computation.2 | async-start | bytes 2228224 | tf_op jit(solution)/shard_map/all_gather | solution.py:171
  34.1 191.3 %all-gather.11.cloned.1.call-start = ((), (), s32[]{:S(2)}) async-start(), calls=%async_computation.4 | async-start | bytes 2228224 | tf_op jit(solution)/shard_map/all_gather | solution.py:31
  43.7 11.4 %copy-start.17 = (f32[64]{0:T(128)S(1)}, f32[64]{0:T(128)}, u32[]{:S(2)}) copy-start(f32[64]{0:T(128)} %param.33) | copy-start | bytes 772
  54.2 0.6 copy-start.3
  54.9 212.2 %reduce-scatter.2.cloned.1.call-start = ((), (), s32[]{:S(2)}) async-start(), calls=%async_computation.3 | async-start | bytes 786432 | tf_op jit(solution)/shard_map/reduce_scatter | solution.py:283
  55.6 5.3 %collective-permute-start = (bf16[64,512]{1,0:T(8,128)(2,1)S(1)}, bf16[64,512]{1,0:T(8,128)(2,1)S(1)}, u32[]{:S(2)}, u32[]{:S(2)}) collective-permute-start(bf16[64,512]{1,0:T(8,128)(2,1)S(1)} %reshape.212), channel_id=1, source_target_pairs={{0,2},{2,0},{4,6},{6,4},{8,10},{10,8},{12,14},{14,12},{16,18},{18,... | collective-permute-start | bytes 196616 | tf_op jit(solution)/shard_map/ppermute | solution.py:26
  60.9 45.7 %collective-permute-start.1 = (bf16[64,512]{1,0:T(8,128)(2,1)S(1)}, bf16[64,512]{1,0:T(8,128)(2,1)S(1)}, u32[]{:S(2)}, u32[]{:S(2)}) collective-permute-start(bf16[64,512]{1,0:T(8,128)(2,1)S(1)} %collective-permute-done), channel_id=1, source_target_pairs={{0,4},{4,0},{2,6},{6,2},{8,12},{12,8},{10,14},{14,10},{16,20},{20,... | collective-permute-start | bytes 196616 | tf_op jit(solution)/shard_map/ppermute | solution.py:26
  106.6 4.3 %collective-permute-start.2 = (bf16[64,512]{1,0:T(8,128)(2,1)S(1)}, bf16[64,512]{1,0:T(8,128)(2,1)S(1)}, u32[]{:S(2)}, u32[]{:S(2)}) collective-permute-start(bf16[64,512]{1,0:T(8,128)(2,1)S(1)} %collective-permute-done.1), channel_id=1, source_target_pairs={{0,8},{8,0},{2,10},{10,2},{4,12},{12,4},{6,14},{14,6},{16,24},{24,... | collective-permute-start | bytes 196616 | tf_op jit(solution)/shard_map/ppermute | solution.py:26
  110.9 53.0 %collective-permute-start.3 = (bf16[64,512]{1,0:T(8,128)(2,1)S(1)}, bf16[64,512]{1,0:T(8,128)(2,1)S(1)}, u32[]{:S(2)}, u32[]{:S(2)}) collective-permute-start(bf16[64,512]{1,0:T(8,128)(2,1)S(1)} %collective-permute-done.2), channel_id=1, source_target_pairs={{0,16},{16,0},{2,18},{18,2},{4,20},{20,4},{6,22},{22,6},{8,24},{24... | collective-permute-start | bytes 196616 | tf_op jit(solution)/shard_map/ppermute | solution.py:26
  166.9 1.6 copy-start.1
  169.4 5.7 %copy-start.15 = (f32[4]{0:T(128)S(1)}, f32[4]{0:T(128)}, u32[]{:S(2)}) copy-start(f32[4]{0:T(128)} %param.35) | copy-start | bytes 52
  169.4 6.2 %copy-start.18 = (f32[128]{0:T(128)S(1)}, f32[128]{0:T(128)}, u32[]{:S(2)}) copy-start(f32[128]{0:T(128)} %param.36) | copy-start | bytes 1540
  172.2 1.6 copy-start.2
  174.7 75.5 %copy-start.11 = (f32[128,512]{0,1:T(8,128)S(1)}, f32[128,512]{0,1:T(8,128)}, u32[]{:S(2)}) copy-start(f32[128,512]{0,1:T(8,128)} %get-tuple-element.532) | copy-start | bytes 786436
  174.7 75.5 %copy-start.19 = (f32[128]{0:T(128)S(1)}, f32[128]{0:T(128)}, u32[]{:S(2)}) copy-start(f32[128]{0:T(128)} %param.45) | copy-start | bytes 1540
  176.0 68.4 %collective-permute-start.4 = (bf16[64,512]{1,0:T(8,128)(2,1)S(1)}, bf16[64,512]{1,0:T(8,128)(2,1)S(1)}, u32[]{:S(2)}, u32[]{:S(2)}) collective-permute-start(bf16[64,512]{1,0:T(8,128)(2,1)S(1)} %bitcast.194), channel_id=1, source_target_pairs={{0,2},{2,0},{4,6},{6,4},{8,10},{10,8},{12,14},{14,12},{16,18},{18,... | collective-permute-start | bytes 196616 | tf_op jit(solution)/shard_map/ppermute | solution.py:26
  242.6 15.5 %copy-start.7 = (bf16[512,2048]{1,0:T(8,128)(2,1)S(1)}, bf16[512,2048]{1,0:T(8,128)(2,1)}, u32[]{:S(2)}) copy-start(bf16[512,2048]{1,0:T(8,128)(2,1)} %param.46) | copy-start | bytes 6291460
  244.4 4.3 %collective-permute-start.5 = (bf16[64,512]{1,0:T(8,128)(2,1)S(1)}, bf16[64,512]{1,0:T(8,128)(2,1)S(1)}, u32[]{:S(2)}, u32[]{:S(2)}) collective-permute-start(bf16[64,512]{1,0:T(8,128)(2,1)S(1)} %collective-permute-done.4), channel_id=1, source_target_pairs={{0,4},{4,0},{2,6},{6,2},{8,12},{12,8},{10,14},{14,10},{16,20},{20,... | collective-permute-start | bytes 196616 | tf_op jit(solution)/shard_map/ppermute | solution.py:26
  248.7 4.3 %collective-permute-start.6 = (bf16[64,512]{1,0:T(8,128)(2,1)S(1)}, bf16[64,512]{1,0:T(8,128)(2,1)S(1)}, u32[]{:S(2)}, u32[]{:S(2)}) collective-permute-start(bf16[64,512]{1,0:T(8,128)(2,1)S(1)} %collective-permute-done.5), channel_id=1, source_target_pairs={{0,8},{8,0},{2,10},{10,2},{4,12},{12,4},{6,14},{14,6},{16,24},{24,... | collective-permute-start | bytes 196616 | tf_op jit(solution)/shard_map/ppermute | solution.py:26
  253.0 5.2 %collective-permute-start.7 = (bf16[64,512]{1,0:T(8,128)(2,1)S(1)}, bf16[64,512]{1,0:T(8,128)(2,1)S(1)}, u32[]{:S(2)}, u32[]{:S(2)}) collective-permute-start(bf16[64,512]{1,0:T(8,128)(2,1)S(1)} %collective-permute-done.6), channel_id=1, source_target_pairs={{0,16},{16,0},{2,18},{18,2},{4,20},{20,4},{6,22},{22,6},{8,24},{24... | collective-permute-start | bytes 196616 | tf_op jit(solution)/shard_map/ppermute | solution.py:26
Sparse Core Ops, SparseCore 0:
  33.4 65.8 all-gather.6
  102.0 61.7 all-gather.8
  166.6 58.7 all-gather.10
  259.6 7.4 reduce-scatter.1
where the time goes:
time: 274 us
  waiting for transfers between devices  124 us (45%)
  blocking collectives  43.2 us (16%)
  other arithmetic  29.7 us (11%)
  local copies, waits for them, and re-layouts  27 us (10%)
  matrix products  23 us (8%)
  between operations  14.8 us (5%)
  starting transfers between devices  11.2 us (4%)
    all_gather x1, waiting for transfers between devices, per_device(): value_rows = lax.all_gather(value_flat, 'sp', axis=0, tiled=True)  52.9 us
    all_gather x1, waiting for transfers between devices, prefix(): everything = jax.tree.map(lambda part: lax.all_gather(part, axis), shard)  47.9 us
    all_gather x1, blocking collectives, prefix(): everything = jax.tree.map(lambda part: lax.all_gather(part, axis), shard)  40.7 us
    select_n x16, other arithmetic, turn(): return jax.tree.map(lambda a, b: jnp.where(reached, a, b), new, before)  16.6 us
    unnamed x52, local copies, waits for them, and re-layouts  15.6 us
    ppermute x8, waiting for transfers between devices, partner(): return lax.ppermute(block, axis, route)  15 us
    ppermute x8, starting transfers between devices, partner(): return lax.ppermute(block, axis, route)  11.1 us
    dot_general x1, matrix products, per_device(): jnp.dot(lax.all_gather(normed, 'tp', axis=0, tiled=True), packed, preferr...  8.26 us
  transfers between devices with their start and end apart: 12, of which 8 were waited for; matrix products, arithmetic and copies ran while one was open for 19% of the time, Pallas kernels for 0%

commit v1 on v0

--- a/solution.py
+++ b/solution.py
@@ -168,7 +168,12 @@
         )
     )
     key_rows = lax.all_gather(key_flat, "sp", axis=0, tiled=True)
-    value_rows = lax.all_gather(value_flat, "sp", axis=0, tiled=True)
+    ring = [value_flat]
+    for hop in range(15):
+        ring.append(lax.ppermute(ring[-1], "sp", [(dev, (dev + 1) % 16) for dev in range(16)]))
+    value_rows = jnp.roll(
+        jnp.concatenate(ring[::-1], axis=0), (lax.axis_index("sp") + 1) * ring[0].shape[0], axis=0
+    )
     piece_rows = key_rows.shape[0]
     span_rows = block_length(piece_rows, row_count)
 

time: 274 us -> 316 us (1.15)
  local copies, waits for them, and re-layouts: 27 us -> 52 us
  waiting for transfers between devices: 124 us -> 148 us
  starting transfers between devices: 11.2 us -> 3.91 us
    ppermute x0 -> x15, waiting for transfers between devices: none -> 121 us  [per_device(): lax.ppermute(ring[-1], 'sp', [(dev, (dev + 1) % 16) for dev in range(16)])]
    all_gather x1 -> x0, waiting for transfers between devices: 52.9 us -> none  [per_device(): value_rows = lax.all_gather(value_flat, 'sp', axis=0, tiled=True)]
    all_gather x1, waiting for transfers between devices: 47.9 us -> 0.02 us  [prefix(): everything = jax.tree.map(lambda part: lax.all_gather(part, axis), shard)]
    unnamed x52 -> x131, local copies, waits for them, and re-layouts: 15.6 us -> 37.9 us
    ppermute x8, starting transfers between devices: 11.1 us -> 0.85 us  [partner(): return lax.ppermute(block, axis, route)]
    ppermute x8, waiting for transfers between devices: 15 us -> 21 us  [partner(): return lax.ppermute(block, axis, route)]
  transfers between devices with their start and end apart: 12 -> 26, of which waited for: 8 -> 22; matrix products, arithmetic and copies ran while one was open for 19% -> 23% of each run, Pallas kernels for 0% -> 0%
where the time goes in v1:
time: 316 us; the launch traced here: 315 us
  waiting for transfers between devices  148 us (47%)
  local copies, waits for them, and re-layouts  52 us (16%)
  blocking collectives  41 us (13%)
  other arithmetic  31.3 us (10%)
  matrix products  22.1 us (7%)
  between operations  15.4 us (5%)
  starting transfers between devices  3.91 us (1%)
    ppermute x15, waiting for transfers between devices, per_device(): lax.ppermute(ring[-1], 'sp', [(dev, (dev + 1) % 16) for dev in range(16)])  121 us
    all_gather x1, blocking collectives, prefix(): everything = jax.tree.map(lambda part: lax.all_gather(part, axis), shard)  38.6 us
    unnamed x131, local copies, waits for them, and re-layouts  37.9 us
    ppermute x8, waiting for transfers between devices, partner(): return lax.ppermute(block, axis, route)  21 us
    select_n x16, other arithmetic, turn(): return jax.tree.map(lambda a, b: jnp.where(reached, a, b), new, before)  16.6 us
    dot_general x1, matrix products, per_device(): jnp.dot(lax.all_gather(normed, 'tp', axis=0, tiled=True), packed, preferr...  8.26 us
    reduce_scatter x1, waiting for transfers between devices, per_device(): lax.psum_scatter((jnp.dot(attn_out, differential_output_rows, preferred_e...  6.71 us
  transfers between devices with their start and end apart: 26, of which 22 were waited for; matrix products, arithmetic and copies ran while one was open for 23% of the time, Pallas kernels for 0%

profile of v1, /device:TPU:0, one launch (start us, length us, event | category | flops | bytes accessed | tf_op | source)
XLA Modules:
  0.0 314.9 jit_solution(1062680917573021336)
XLA Ops:
  6.6 3.2 %constant_dynamic-update-slice_fusion.7 = bf16[2048,3104]{1,0:T(8,128)(2,1)} fusion(bf16[2048,512]{1,0:T(8,128)(2,1)} %param.30), kind=kLoop, calls=%fused_computation.125 | loop fusion | bytes 4194304
  10.4 2.4 all_gather.18
  12.9 3.3 %constant_dynamic-update-slice_fusion.6 = bf16[2048,3104]{1,0:T(8,128)(2,1)} fusion(bf16[2048,3104]{1,0:T(8,128)(2,1)} %constant_dynamic-update-slice_fusion.7, bf16[2048,512]{1,0:T(8,128)(2,1)} %param.31), kind=kLoop, calls=%fused_computation.124 | loop fusion | bytes 4194304
  16.2 1.5 constant_dynamic-update-slice_fusion.5
  17.7 1.1 constant_dynamic-update-slice_fusion.4
  20.0 1.5 constant_dynamic-update-slice_fusion.2
  21.5 1.5 constant_dynamic-update-slice_fusion.1
  24.0 8.3 %convolution_convert_fusion = bf16[128,3104]{0,1:T(8,128)(2,1)S(1)} fusion(bf16[128,2048]{1,0:T(8,128)(2,1)S(1)} %all_gather.18, bf16[2048,3104]{1,0:T(8,128)(2,1)} %constant_dynamic-update-slice_fusion), kind=kOutput, calls=%fused_computation.68 | convolution fusion | flops 1627787264 | bytes 14032896 | tf_op jit(solution)/shard_map/dot_general | solution.py:131
  32.2 2.9 collective-permute-start
  35.1 7.8 %collective-permute-done = bf16[128,512]{0,1:T(8,128)(2,1)S(1)} collective-permute-done((bf16[128,512]{0,1:T(8,128)(2,1)S(1)}, bf16[128,512]{0,1:T(8,128)(2,1)S(1)}, u32[]{:S(2)}, u32[]{:S(2)}) %collective-permute-start) | collective-permute-done | bytes 131104 | tf_op jit(solution)/shard_map/ppermute | solution.py:173
  43.6 8.6 %collective-permute-done.1 = bf16[128,512]{0,1:T(8,128)(2,1)S(1)} collective-permute-done((bf16[128,512]{0,1:T(8,128)(2,1)S(1)}, bf16[128,512]{0,1:T(8,128)(2,1)S(1)}, u32[]{:S(2)}, u32[]{:S(2)}) %collective-permute-start.1) | collective-permute-done | bytes 131104 | tf_op jit(solution)/shard_map/ppermute | solution.py:173
  52.8 8.6 %collective-permute-done.2 = bf16[128,512]{0,1:T(8,128)(2,1)S(1)} collective-permute-done((bf16[128,512]{0,1:T(8,128)(2,1)S(1)}, bf16[128,512]{0,1:T(8,128)(2,1)S(1)}, u32[]{:S(2)}, u32[]{:S(2)}) %collective-permute-start.2) | collective-permute-done | bytes 131104 | tf_op jit(solution)/shard_map/ppermute | solution.py:173
  62.0 8.6 %collective-permute-done.3 = bf16[128,512]{0,1:T(8,128)(2,1)S(1)} collective-permute-done((bf16[128,512]{0,1:T(8,128)(2,1)S(1)}, bf16[128,512]{0,1:T(8,128)(2,1)S(1)}, u32[]{:S(2)}, u32[]{:S(2)}) %collective-permute-start.3) | collective-permute-done | bytes 131104 | tf_op jit(solution)/shard_map/ppermute | solution.py:173
  71.2 8.6 %collective-permute-done.4 = bf16[128,512]{0,1:T(8,128)(2,1)S(1)} collective-permute-done((bf16[128,512]{0,1:T(8,128)(2,1)S(1)}, bf16[128,512]{0,1:T(8,128)(2,1)S(1)}, u32[]{:S(2)}, u32[]{:S(2)}) %collective-permute-start.4) | collective-permute-done | bytes 131104 | tf_op jit(solution)/shard_map/ppermute | solution.py:173
  80.5 8.6 %collective-permute-done.5 = bf16[128,512]{0,1:T(8,128)(2,1)S(1)} collective-permute-done((bf16[128,512]{0,1:T(8,128)(2,1)S(1)}, bf16[128,512]{0,1:T(8,128)(2,1)S(1)}, u32[]{:S(2)}, u32[]{:S(2)}) %collective-permute-start.5) | collective-permute-done | bytes 131104 | tf_op jit(solution)/shard_map/ppermute | solution.py:173
  89.7 9.1 %collective-permute-done.6 = bf16[128,512]{0,1:T(8,128)(2,1)S(1)} collective-permute-done((bf16[128,512]{0,1:T(8,128)(2,1)S(1)}, bf16[128,512]{0,1:T(8,128)(2,1)S(1)}, u32[]{:S(2)}, u32[]{:S(2)}) %collective-permute-start.6) | collective-permute-done | bytes 131104 | tf_op jit(solution)/shard_map/ppermute | solution.py:173
  99.4 9.7 %collective-permute-done.7 = bf16[128,512]{0,1:T(8,128)(2,1)S(1)} collective-permute-done((bf16[128,512]{0,1:T(8,128)(2,1)S(1)}, bf16[128,512]{0,1:T(8,128)(2,1)S(1)}, u32[]{:S(2)}, u32[]{:S(2)}) %collective-permute-start.7) | collective-permute-done | bytes 131104 | tf_op jit(solution)/shard_map/ppermute | solution.py:173
  109.8 8.6 %collective-permute-done.8 = bf16[128,512]{0,1:T(8,128)(2,1)S(1)} collective-permute-done((bf16[128,512]{0,1:T(8,128)(2,1)S(1)}, bf16[128,512]{0,1:T(8,128)(2,1)S(1)}, u32[]{:S(2)}, u32[]{:S(2)}) %collective-permute-start.8) | collective-permute-done | bytes 131104 | tf_op jit(solution)/shard_map/ppermute | solution.py:173
  118.5 8.4 %collective-permute-done.9 = bf16[128,512]{0,1:T(8,128)(2,1)S(1)} collective-permute-done((bf16[128,512]{0,1:T(8,128)(2,1)S(1)}, bf16[128,512]{0,1:T(8,128)(2,1)S(1)}, u32[]{:S(2)}, u32[]{:S(2)}) %collective-permute-start.9) | collective-permute-done | bytes 131104 | tf_op jit(solution)/shard_map/ppermute | solution.py:173
  128.0 7.5 %collective-permute-done.10 = bf16[128,512]{0,1:T(8,128)(2,1)S(1)} collective-permute-done((bf16[128,512]{0,1:T(8,128)(2,1)S(1)}, bf16[128,512]{0,1:T(8,128)(2,1)S(1)}, u32[]{:S(2)}, u32[]{:S(2)}) %collective-permute-start.10) | collective-permute-done | bytes 131104 | tf_op jit(solution)/shard_map/ppermute | solution.py:173
  137.5 1.4 copy.134
  138.9 5.4 %collective-permute-done.11 = bf16[128,512]{0,1:T(8,128)(2,1)} collective-permute-done((bf16[128,512]{0,1:T(8,128)(2,1)S(1)}, bf16[128,512]{0,1:T(8,128)(2,1)}, u32[]{:S(2)}, u32[]{:S(2)}) %collective-permute-start.11) | collective-permute-done | bytes 131104 | tf_op jit(solution)/shard_map/ppermute | solution.py:173
  146.0 7.1 %collective-permute-done.12 = bf16[128,512]{0,1:T(8,128)(2,1)} collective-permute-done((bf16[128,512]{0,1:T(8,128)(2,1)}, bf16[128,512]{0,1:T(8,128)(2,1)}, u32[]{:S(2)}, u32[]{:S(2)}) %collective-permute-start.12) | collective-permute-done | bytes 131104 | tf_op jit(solution)/shard_map/ppermute | solution.py:173
  153.8 1.8 reshape.219
  155.7 7.2 %collective-permute-done.13 = bf16[128,512]{0,1:T(8,128)(2,1)} collective-permute-done((bf16[128,512]{0,1:T(8,128)(2,1)}, bf16[128,512]{0,1:T(8,128)(2,1)}, u32[]{:S(2)}, u32[]{:S(2)}) %collective-permute-start.13) | collective-permute-done | bytes 131104 | tf_op jit(solution)/shard_map/ppermute | solution.py:173
  162.9 1.7 broadcast_add_fusion
  164.7 7.0 %collective-permute-done.14 = bf16[128,512]{0,1:T(8,128)(2,1)S(1)} collective-permute-done((bf16[128,512]{0,1:T(8,128)(2,1)}, bf16[128,512]{0,1:T(8,128)(2,1)S(1)}, u32[]{:S(2)}, u32[]{:S(2)}) %collective-permute-start.14) | collective-permute-done | bytes 131104 | tf_op jit(solution)/shard_map/ppermute | solution.py:173
  188.5 2.0 copy-done.8
  191.0 10.5 %while.8 = (s32[]{:T(128)}, f32[4,64,128]{2,1,0:T(8,128)S(1)}, f32[4,64]{1,0:T(4,128)S(1)}, f32[2,64,4,128]{3,1,0,2:T(8,128)}, f32[2,64,4,64]{3,2,1,0:T(4,128)},...) while((s32[]{:T(128)}, f32[4,64,128]{2,1,0:T(8,128)S(1)}, ...), condition=%wide.region_17.18_spmd.clone, body=%wide.region_15.17_spmd.clone.sunk | while | flops 89412096 | bytes 2970753 | solution.py:261
  191.0 1.3 constant_dynamic-slice_fusion.4
  196.2 1.2 constant_dynamic-slice_fusion.4
  205.7 2.2 collective-permute-done.15
  207.8 4.3 %collective-permute-done.16 = bf16[64,512]{1,0:T(8,128)(2,1)S(1)} collective-permute-done((bf16[64,512]{1,0:T(8,128)(2,1)S(1)}, bf16[64,512]{1,0:T(8,128)(2,1)S(1)}, u32[]{:S(2)}, u32[]{:S(2)}) %collective-permute-start.16) | collective-permute-done | bytes 65568 | tf_op jit(solution)/shard_map/ppermute | solution.py:26
  212.1 4.7 %collective-permute-done.17 = bf16[64,512]{1,0:T(8,128)(2,1)S(1)} collective-permute-done((bf16[64,512]{1,0:T(8,128)(2,1)S(1)}, bf16[64,512]{1,0:T(8,128)(2,1)S(1)}, u32[]{:S(2)}, u32[]{:S(2)}) %collective-permute-start.17) | collective-permute-done | bytes 65568 | tf_op jit(solution)/shard_map/ppermute | solution.py:26
  216.8 3.1 constant_dynamic-slice_fusion.2
  219.9 2.0 collective-permute-done.18
  221.9 5.4 %conditional.3 = (f32[8,64]{1,0:T(8,128)S(1)}, f32[8,64,128]{2,1,0:T(8,128)S(1)}) conditional(s32[]{:T(128)} %convert_element_type.81, (f32[8,64]{1,0:T(8,128)S(1)}, f32[8,64,128]{2,1,0:T(8,128)S(1)}) %tuple.49, (s32[2048]{0:T(1024)S(1)}, s32[64]{0:T(128)S(1)}, bf16[64,512]{1,0:T(8,128)(2,1)S(1)}, bf16[2048,8,64]{0,2,1:T(8,128)(2,1)}, ...), branch_computations={%region_10.11_spmd, %region_11.14_spmd} | conditional | flops 412353536 | bytes 26839340 | solution.py:192
  222.2 2.7 fusion.9
  224.9 1.3 fusion.10
  227.4 5.3 %conditional.2 = ((f32[8,64]{1,0:T(8,128)S(1)}, f32[8,64,128]{2,1,0:T(8,128)S(1)})) conditional(s32[]{:T(128)} %convert_element_type.71, (f32[8,64]{1,0:T(8,128)S(1)}, f32[8,64,128]{2,1,0:T(8,128)S(1)}) %tuple.49, (s32[2048]{0:T(1024)S(1)}, s32[64]{0:T(128)S(1)}, bf16[128,8,64]{2,0,1:T(8,128)(2,1)S(1)}, bf16[2048,8,64]{0,2,1:T(8,128)(2,1)}, ...), branch_computations={%region_4.5_spmd, %region_5.0_spmd} | conditional | flops 412353536 | bytes 26773812 | solution.py:192
  227.6 2.6 fusion.2
  230.2 1.3 fusion.3
  234.6 3.7 %collective-permute-done.19 = bf16[64,512]{1,0:T(8,128)(2,1)S(1)} collective-permute-done((bf16[64,512]{1,0:T(8,128)(2,1)S(1)}, bf16[64,512]{1,0:T(8,128)(2,1)S(1)}, u32[]{:S(2)}, u32[]{:S(2)}) %collective-permute-start.19) | collective-permute-done | bytes 65568 | tf_op jit(solution)/shard_map/ppermute | solution.py:26
  238.4 4.2 %collective-permute-done.20 = bf16[64,512]{1,0:T(8,128)(2,1)S(1)} collective-permute-done((bf16[64,512]{1,0:T(8,128)(2,1)S(1)}, bf16[64,512]{1,0:T(8,128)(2,1)S(1)}, u32[]{:S(2)}, u32[]{:S(2)}) %collective-permute-start.20) | collective-permute-done | bytes 65568 | tf_op jit(solution)/shard_map/ppermute | solution.py:26
  242.8 38.6 %all-gather.2 = f32[16,4,64]{2,1,0:T(4,128)S(1)} all-gather(f32[1,4,64]{2,1,0:T(4,128)S(1)} %exponential_bitcast_fusion), channel_id=2, replica_groups=mesh['sp'=16,'tp'=2] {'sp'}, dimensions={0}, use_global_device_ids=true | all-gather | bytes 17408 | tf_op jit(solution)/shard_map/all_gather | solution.py:31
  281.5 17.3 %while.9 = (s32[]{:T(128)}, f32[4,64,128]{2,1,0:T(8,128)S(1)}, s32[]{:T(128)}, f32[16,4,64]{2,1,0:T(4,128)S(1)}, f32[16,4,64,128]{3,2,1,0:T(8,128)}, /*index=5*/s32[]{:T(128)}, s32[]{:T(128)}) while((s32[]{:T(128)}, f32[4,64,128]{2,1,0:T(8,128)S(1)}, s32[]{:T(128)}, f32[16,4,64]{2,1,0:T(4,128)S(1)}, ...), condition=%wide.region_19.20_spmd.clone, body=%wide.region_18.19_spmd.clone.sunk | while | flops 131076 | bytes 396393 | solution.py:43
  300.4 1.3 fusion.41
  301.6 6.7 %reduce-scatter.2.cloned.1.call-done = bf16[64,2048]{1,0:T(8,128)(2,1)} async-done(((bf16[128,2048]{1,0:T(8,128)(2,1)}), bf16[64,2048]{1,0:T(8,128)(2,1)}) %reduce-scatter.2.cloned.1.call-update) | async-done | bytes 262160 | tf_op jit(solution)/shard_map/reduce_scatter | solution.py:288
  (276 shorter events, 64.1 us)
Async XLA Ops:
  6.5 293.0 %copy-start = (bf16[512,2048]{1,0:T(8,128)(2,1)S(1)}, bf16[512,2048]{1,0:T(8,128)(2,1)}, u32[]{:S(2)}) copy-start(bf16[512,2048]{1,0:T(8,128)(2,1)} %param.47) | copy-start | bytes 6291460
  6.5 213.4 %all-gather.6.cloned.1.call-start = ((), (), s32[]{:S(2)}) async-start(), calls=%async_computation.1 | async-start | bytes 2228224 | tf_op jit(solution)/shard_map/all_gather | solution.py:170
  23.9 94.4 %copy-start.41 = (f32[64]{0:T(128)S(1)}, f32[64]{0:T(128)}, u32[]{:S(2)}) copy-start(f32[64]{0:T(128)} %param.34) | copy-start | bytes 772
  24.0 111.5 %copy-start.44 = (bf16[32,256]{1,0:T(8,128)(2,1)S(1)}, bf16[32,256]{1,0:T(8,128)(2,1)}, u32[]{:S(2)}) copy-start(bf16[32,256]{1,0:T(8,128)(2,1)} %param.42) | copy-start | bytes 49156
  24.0 111.6 %copy-start.45 = (f32[256]{0:T(256)S(1)}, f32[256]{0:T(256)}, u32[]{:S(2)}) copy-start(f32[256]{0:T(256)} %param.43) | copy-start | bytes 3076
  32.2 10.7 %collective-permute-start = (bf16[128,512]{0,1:T(8,128)(2,1)S(1)}, bf16[128,512]{0,1:T(8,128)(2,1)S(1)}, u32[]{:S(2)}, u32[]{:S(2)}) collective-permute-start(bf16[128,512]{0,1:T(8,128)(2,1)S(1)} %slice.63), channel_id=1, source_target_pairs={{0,2},{2,4},{4,6},{6,8},{8,10},{10,12},{12,14},{14,16},{16,18},{18... | collective-permute-start | bytes 393224 | tf_op jit(solution)/shard_map/ppermute | solution.py:173
  43.6 8.6 %collective-permute-start.1 = (bf16[128,512]{0,1:T(8,128)(2,1)S(1)}, bf16[128,512]{0,1:T(8,128)(2,1)S(1)}, u32[]{:S(2)}, u32[]{:S(2)}) collective-permute-start(bf16[128,512]{0,1:T(8,128)(2,1)S(1)} %collective-permute-done), channel_id=1, source_target_pairs={{0,2},{2,4},{4,6},{6,8},{8,10},{10,12},{12,14},{14,16},{16,18},{18... | collective-permute-start | bytes 393224 | tf_op jit(solution)/shard_map/ppermute | solution.py:173
  52.8 8.6 %collective-permute-start.2 = (bf16[128,512]{0,1:T(8,128)(2,1)S(1)}, bf16[128,512]{0,1:T(8,128)(2,1)S(1)}, u32[]{:S(2)}, u32[]{:S(2)}) collective-permute-start(bf16[128,512]{0,1:T(8,128)(2,1)S(1)} %collective-permute-done.1), channel_id=1, source_target_pairs={{0,2},{2,4},{4,6},{6,8},{8,10},{10,12},{12,14},{14,16},{16,18},{18... | collective-permute-start | bytes 393224 | tf_op jit(solution)/shard_map/ppermute | solution.py:173
  62.0 8.6 %collective-permute-start.3 = (bf16[128,512]{0,1:T(8,128)(2,1)S(1)}, bf16[128,512]{0,1:T(8,128)(2,1)S(1)}, u32[]{:S(2)}, u32[]{:S(2)}) collective-permute-start(bf16[128,512]{0,1:T(8,128)(2,1)S(1)} %collective-permute-done.2), channel_id=1, source_target_pairs={{0,2},{2,4},{4,6},{6,8},{8,10},{10,12},{12,14},{14,16},{16,18},{18... | collective-permute-start | bytes 393224 | tf_op jit(solution)/shard_map/ppermute | solution.py:173
  71.2 8.6 %collective-permute-start.4 = (bf16[128,512]{0,1:T(8,128)(2,1)S(1)}, bf16[128,512]{0,1:T(8,128)(2,1)S(1)}, u32[]{:S(2)}, u32[]{:S(2)}) collective-permute-start(bf16[128,512]{0,1:T(8,128)(2,1)S(1)} %collective-permute-done.3), channel_id=1, source_target_pairs={{0,2},{2,4},{4,6},{6,8},{8,10},{10,12},{12,14},{14,16},{16,18},{18... | collective-permute-start | bytes 393224 | tf_op jit(solution)/shard_map/ppermute | solution.py:173
  80.5 8.6 %collective-permute-start.5 = (bf16[128,512]{0,1:T(8,128)(2,1)S(1)}, bf16[128,512]{0,1:T(8,128)(2,1)S(1)}, u32[]{:S(2)}, u32[]{:S(2)}) collective-permute-start(bf16[128,512]{0,1:T(8,128)(2,1)S(1)} %collective-permute-done.4), channel_id=1, source_target_pairs={{0,2},{2,4},{4,6},{6,8},{8,10},{10,12},{12,14},{14,16},{16,18},{18... | collective-permute-start | bytes 393224 | tf_op jit(solution)/shard_map/ppermute | solution.py:173
  89.7 9.1 %collective-permute-start.6 = (bf16[128,512]{0,1:T(8,128)(2,1)S(1)}, bf16[128,512]{0,1:T(8,128)(2,1)S(1)}, u32[]{:S(2)}, u32[]{:S(2)}) collective-permute-start(bf16[128,512]{0,1:T(8,128)(2,1)S(1)} %collective-permute-done.5), channel_id=1, source_target_pairs={{0,2},{2,4},{4,6},{6,8},{8,10},{10,12},{12,14},{14,16},{16,18},{18... | collective-permute-start | bytes 393224 | tf_op jit(solution)/shard_map/ppermute | solution.py:173
  99.4 9.7 %collective-permute-start.7 = (bf16[128,512]{0,1:T(8,128)(2,1)S(1)}, bf16[128,512]{0,1:T(8,128)(2,1)S(1)}, u32[]{:S(2)}, u32[]{:S(2)}) collective-permute-start(bf16[128,512]{0,1:T(8,128)(2,1)S(1)} %collective-permute-done.6), channel_id=1, source_target_pairs={{0,2},{2,4},{4,6},{6,8},{8,10},{10,12},{12,14},{14,16},{16,18},{18... | collective-permute-start | bytes 393224 | tf_op jit(solution)/shard_map/ppermute | solution.py:173
  109.8 8.6 %collective-permute-start.8 = (bf16[128,512]{0,1:T(8,128)(2,1)S(1)}, bf16[128,512]{0,1:T(8,128)(2,1)S(1)}, u32[]{:S(2)}, u32[]{:S(2)}) collective-permute-start(bf16[128,512]{0,1:T(8,128)(2,1)S(1)} %collective-permute-done.7), channel_id=1, source_target_pairs={{0,2},{2,4},{4,6},{6,8},{8,10},{10,12},{12,14},{14,16},{16,18},{18... | collective-permute-start | bytes 393224 | tf_op jit(solution)/shard_map/ppermute | solution.py:173
  118.4 9.6 %copy-start.30 = (bf16[128,512]{0,1:T(8,128)(2,1)}, bf16[128,512]{0,1:T(8,128)(2,1)S(1)}, u32[]{:S(2)}) copy-start(bf16[128,512]{0,1:T(8,128)(2,1)S(1)} %collective-permute-done.8) | copy-start | bytes 393220
  118.4 8.6 %collective-permute-start.9 = (bf16[128,512]{0,1:T(8,128)(2,1)S(1)}, bf16[128,512]{0,1:T(8,128)(2,1)S(1)}, u32[]{:S(2)}, u32[]{:S(2)}) collective-permute-start(bf16[128,512]{0,1:T(8,128)(2,1)S(1)} %collective-permute-done.8), channel_id=1, source_target_pairs={{0,2},{2,4},{4,6},{6,8},{8,10},{10,12},{12,14},{14,16},{16,18},{18... | collective-permute-start | bytes 393224 | tf_op jit(solution)/shard_map/ppermute | solution.py:173
  126.9 17.3 %copy-start.32 = (bf16[128,512]{0,1:T(8,128)(2,1)}, bf16[128,512]{0,1:T(8,128)(2,1)S(1)}, u32[]{:S(2)}) copy-start(bf16[128,512]{0,1:T(8,128)(2,1)S(1)} %collective-permute-done.9) | copy-start | bytes 393220
  126.9 8.6 %collective-permute-start.10 = (bf16[128,512]{0,1:T(8,128)(2,1)S(1)}, bf16[128,512]{0,1:T(8,128)(2,1)S(1)}, u32[]{:S(2)}, u32[]{:S(2)}) collective-permute-start(bf16[128,512]{0,1:T(8,128)(2,1)S(1)} %collective-permute-done.9), channel_id=1, source_target_pairs={{0,2},{2,4},{4,6},{6,8},{8,10},{10,12},{12,14},{14,16},{16,18},{18... | collective-permute-start | bytes 393224 | tf_op jit(solution)/shard_map/ppermute | solution.py:173
  127.9 153.6 %all-gather.8.cloned.1.call-start = ((), (), s32[]{:S(2)}) async-start(), calls=%async_computation.3 | async-start | bytes 2228224 | tf_op jit(solution)/shard_map/all_gather | solution.py:31
  135.5 8.8 %collective-permute-start.11 = (bf16[128,512]{0,1:T(8,128)(2,1)S(1)}, bf16[128,512]{0,1:T(8,128)(2,1)}, u32[]{:S(2)}, u32[]{:S(2)}) collective-permute-start(bf16[128,512]{0,1:T(8,128)(2,1)S(1)} %collective-permute-done.10), channel_id=1, source_target_pairs={{0,2},{2,4},{4,6},{6,8},{8,10},{10,12},{12,14},{14,16},{16,18},{18... | collective-permute-start | bytes 393224 | tf_op jit(solution)/shard_map/ppermute | solution.py:173
  144.3 8.9 %collective-permute-start.12 = (bf16[128,512]{0,1:T(8,128)(2,1)}, bf16[128,512]{0,1:T(8,128)(2,1)}, u32[]{:S(2)}, u32[]{:S(2)}) collective-permute-start(bf16[128,512]{0,1:T(8,128)(2,1)} %collective-permute-done.11), channel_id=1, source_target_pairs={{0,2},{2,4},{4,6},{6,8},{8,10},{10,12},{12,14},{14,16},{16,18},{18... | collective-permute-start | bytes 393224 | tf_op jit(solution)/shard_map/ppermute | solution.py:173
  153.1 9.8 %collective-permute-start.13 = (bf16[128,512]{0,1:T(8,128)(2,1)}, bf16[128,512]{0,1:T(8,128)(2,1)}, u32[]{:S(2)}, u32[]{:S(2)}) collective-permute-start(bf16[128,512]{0,1:T(8,128)(2,1)} %collective-permute-done.12), channel_id=1, source_target_pairs={{0,2},{2,4},{4,6},{6,8},{8,10},{10,12},{12,14},{14,16},{16,18},{18... | collective-permute-start | bytes 393224 | tf_op jit(solution)/shard_map/ppermute | solution.py:173
  155.6 28.5 %copy-start.15 = (bf16[128,512]{0,1:T(8,128)(2,1)S(1)}, bf16[128,512]{0,1:T(8,128)(2,1)}, u32[]{:S(2)}) copy-start(bf16[128,512]{0,1:T(8,128)(2,1)} %copy-done.14) | copy-start | bytes 393220
  155.6 31.5 %copy-start.35 = (bf16[128,512]{0,1:T(8,128)(2,1)S(1)}, bf16[128,512]{0,1:T(8,128)(2,1)}, u32[]{:S(2)}) copy-start(bf16[128,512]{0,1:T(8,128)(2,1)} %copy-done.34) | copy-start | bytes 393220
  155.6 31.6 %copy-start.33 = (bf16[128,512]{0,1:T(8,128)(2,1)S(1)}, bf16[128,512]{0,1:T(8,128)(2,1)}, u32[]{:S(2)}) copy-start(bf16[128,512]{0,1:T(8,128)(2,1)} %copy-done.32) | copy-start | bytes 393220
  155.6 31.6 %copy-start.31 = (bf16[128,512]{0,1:T(8,128)(2,1)S(1)}, bf16[128,512]{0,1:T(8,128)(2,1)}, u32[]{:S(2)}) copy-start(bf16[128,512]{0,1:T(8,128)(2,1)} %copy-done.30) | copy-start | bytes 393220
  155.6 31.7 %copy-start.29 = (bf16[128,512]{0,1:T(8,128)(2,1)S(1)}, bf16[128,512]{0,1:T(8,128)(2,1)}, u32[]{:S(2)}) copy-start(bf16[128,512]{0,1:T(8,128)(2,1)} %copy-done.28) | copy-start | bytes 393220
  155.6 31.7 %copy-start.27 = (bf16[128,512]{0,1:T(8,128)(2,1)S(1)}, bf16[128,512]{0,1:T(8,128)(2,1)}, u32[]{:S(2)}) copy-start(bf16[128,512]{0,1:T(8,128)(2,1)} %copy-done.26) | copy-start | bytes 393220
  155.6 31.8 %copy-start.25 = (bf16[128,512]{0,1:T(8,128)(2,1)S(1)}, bf16[128,512]{0,1:T(8,128)(2,1)}, u32[]{:S(2)}) copy-start(bf16[128,512]{0,1:T(8,128)(2,1)} %copy-done.24) | copy-start | bytes 393220
  155.7 31.8 %copy-start.23 = (bf16[128,512]{0,1:T(8,128)(2,1)S(1)}, bf16[128,512]{0,1:T(8,128)(2,1)}, u32[]{:S(2)}) copy-start(bf16[128,512]{0,1:T(8,128)(2,1)} %copy-done.22) | copy-start | bytes 393220
  155.7 31.9 %copy-start.21 = (bf16[128,512]{0,1:T(8,128)(2,1)S(1)}, bf16[128,512]{0,1:T(8,128)(2,1)}, u32[]{:S(2)}) copy-start(bf16[128,512]{0,1:T(8,128)(2,1)} %copy-done.20) | copy-start | bytes 393220
  155.7 31.9 %copy-start.19 = (bf16[128,512]{0,1:T(8,128)(2,1)S(1)}, bf16[128,512]{0,1:T(8,128)(2,1)}, u32[]{:S(2)}) copy-start(bf16[128,512]{0,1:T(8,128)(2,1)} %copy-done.18) | copy-start | bytes 393220
  155.7 32.0 %copy-start.17 = (bf16[128,512]{0,1:T(8,128)(2,1)S(1)}, bf16[128,512]{0,1:T(8,128)(2,1)}, u32[]{:S(2)}) copy-start(bf16[128,512]{0,1:T(8,128)(2,1)} %copy-done.16) | copy-start | bytes 393220
  162.9 8.8 %collective-permute-start.14 = (bf16[128,512]{0,1:T(8,128)(2,1)}, bf16[128,512]{0,1:T(8,128)(2,1)S(1)}, u32[]{:S(2)}, u32[]{:S(2)}) collective-permute-start(bf16[128,512]{0,1:T(8,128)(2,1)} %collective-permute-done.13), channel_id=1, source_target_pairs={{0,2},{2,4},{4,6},{6,8},{8,10},{10,12},{12,14},{14,16},{16,18},{18... | collective-permute-start | bytes 393224 | tf_op jit(solution)/shard_map/ppermute | solution.py:173
  191.0 11.2 %copy-start.13 = (bf16[128,512]{0,1:T(8,128)(2,1)S(1)}, bf16[128,512]{0,1:T(8,128)(2,1)}, u32[]{:S(2)}) copy-start(bf16[128,512]{0,1:T(8,128)(2,1)} %get-tuple-element.514) | copy-start | bytes 393220
  202.1 106.2 %reduce-scatter.2.cloned.1.call-start = ((), (), s32[]{:S(2)}) async-start(), calls=%async_computation.2 | async-start | bytes 786432 | tf_op jit(solution)/shard_map/reduce_scatter | solution.py:288
  203.5 4.3 %collective-permute-start.15 = (bf16[64,512]{1,0:T(8,128)(2,1)S(1)}, bf16[64,512]{1,0:T(8,128)(2,1)S(1)}, u32[]{:S(2)}, u32[]{:S(2)}) collective-permute-start(bf16[64,512]{1,0:T(8,128)(2,1)S(1)} %reshape.212), channel_id=1, source_target_pairs={{0,2},{2,0},{4,6},{6,4},{8,10},{10,8},{12,14},{14,12},{16,18},{18,... | collective-permute-start | bytes 196616 | tf_op jit(solution)/shard_map/ppermute | solution.py:26
  207.8 4.3 %collective-permute-start.16 = (bf16[64,512]{1,0:T(8,128)(2,1)S(1)}, bf16[64,512]{1,0:T(8,128)(2,1)S(1)}, u32[]{:S(2)}, u32[]{:S(2)}) collective-permute-start(bf16[64,512]{1,0:T(8,128)(2,1)S(1)} %collective-permute-done.15), channel_id=1, source_target_pairs={{0,4},{4,0},{2,6},{6,2},{8,12},{12,8},{10,14},{14,10},{16,20},{20,... | collective-permute-start | bytes 196616 | tf_op jit(solution)/shard_map/ppermute | solution.py:26
  212.1 4.7 %collective-permute-start.17 = (bf16[64,512]{1,0:T(8,128)(2,1)S(1)}, bf16[64,512]{1,0:T(8,128)(2,1)S(1)}, u32[]{:S(2)}, u32[]{:S(2)}) collective-permute-start(bf16[64,512]{1,0:T(8,128)(2,1)S(1)} %collective-permute-done.16), channel_id=1, source_target_pairs={{0,8},{8,0},{2,10},{10,2},{4,12},{12,4},{6,14},{14,6},{16,24},{24,... | collective-permute-start | bytes 196616 | tf_op jit(solution)/shard_map/ppermute | solution.py:26
  216.8 5.2 %collective-permute-start.18 = (bf16[64,512]{1,0:T(8,128)(2,1)S(1)}, bf16[64,512]{1,0:T(8,128)(2,1)S(1)}, u32[]{:S(2)}, u32[]{:S(2)}) collective-permute-start(bf16[64,512]{1,0:T(8,128)(2,1)S(1)} %collective-permute-done.17), channel_id=1, source_target_pairs={{0,16},{16,0},{2,18},{18,2},{4,20},{20,4},{6,22},{22,6},{8,24},{24... | collective-permute-start | bytes 196616 | tf_op jit(solution)/shard_map/ppermute | solution.py:26
  227.4 15.2 %copy-start.37 = (f32[2,64,4,128]{3,1,0,2:T(8,128)S(1)}, f32[2,64,4,128]{3,1,0,2:T(8,128)}, u32[]{:S(2)}) copy-start(f32[2,64,4,128]{3,1,0,2:T(8,128)} %get-tuple-element.296) | copy-start | bytes 786436
  232.7 66.1 %copy-start.36 = (f32[2,64,4,64]{3,2,1,0:T(4,128)S(1)}, f32[2,64,4,64]{3,2,1,0:T(4,128)}, u32[]{:S(2)}) copy-start(f32[2,64,4,64]{3,2,1,0:T(4,128)} %get-tuple-element.300) | copy-start | bytes 393220
  232.7 66.7 %copy-start.12 = (f32[128,512]{0,1:T(8,128)S(1)}, f32[128,512]{0,1:T(8,128)}, u32[]{:S(2)}) copy-start(f32[128,512]{0,1:T(8,128)} %get-tuple-element.516) | copy-start | bytes 786436
  232.7 66.7 %copy-start.43 = (f32[128]{0:T(128)S(1)}, f32[128]{0:T(128)}, u32[]{:S(2)}) copy-start(f32[128]{0:T(128)} %param.45) | copy-start | bytes 1540
  234.0 4.4 %collective-permute-start.19 = (bf16[64,512]{1,0:T(8,128)(2,1)S(1)}, bf16[64,512]{1,0:T(8,128)(2,1)S(1)}, u32[]{:S(2)}, u32[]{:S(2)}) collective-permute-start(bf16[64,512]{1,0:T(8,128)(2,1)S(1)} %bitcast.194), channel_id=1, source_target_pairs={{0,2},{2,0},{4,6},{6,4},{8,10},{10,8},{12,14},{14,12},{16,18},{18,... | collective-permute-start | bytes 196616 | tf_op jit(solution)/shard_map/ppermute | solution.py:26
  238.3 4.3 %collective-permute-start.20 = (bf16[64,512]{1,0:T(8,128)(2,1)S(1)}, bf16[64,512]{1,0:T(8,128)(2,1)S(1)}, u32[]{:S(2)}, u32[]{:S(2)}) collective-permute-start(bf16[64,512]{1,0:T(8,128)(2,1)S(1)} %collective-permute-done.19), channel_id=1, source_target_pairs={{0,4},{4,0},{2,6},{6,2},{8,12},{12,8},{10,14},{14,10},{16,20},{20,... | collective-permute-start | bytes 196616 | tf_op jit(solution)/shard_map/ppermute | solution.py:26
  242.6 38.8 %collective-permute-start.21 = (bf16[64,512]{1,0:T(8,128)(2,1)S(1)}, bf16[64,512]{1,0:T(8,128)(2,1)}, u32[]{:S(2)}, u32[]{:S(2)}) collective-permute-start(bf16[64,512]{1,0:T(8,128)(2,1)S(1)} %collective-permute-done.20), channel_id=1, source_target_pairs={{0,8},{8,0},{2,10},{10,2},{4,12},{12,4},{6,14},{14,6},{16,24},{24,... | collective-permute-start | bytes 196616 | tf_op jit(solution)/shard_map/ppermute | solution.py:26
  281.4 18.7 %collective-permute-start.22 = (bf16[64,512]{1,0:T(8,128)(2,1)}, bf16[64,512]{1,0:T(8,128)(2,1)S(1)}, u32[]{:S(2)}, u32[]{:S(2)}) collective-permute-start(bf16[64,512]{1,0:T(8,128)(2,1)} %collective-permute-done.21), channel_id=1, source_target_pairs={{0,16},{16,0},{2,18},{18,2},{4,20},{20,4},{6,22},{22,6},{8,24},{24... | collective-permute-start | bytes 196616 | tf_op jit(solution)/shard_map/ppermute | solution.py:26
  (24 other events, 65.1 us)
Sparse Core Ops, SparseCore 0:
  128.0 66.5 all-gather.5
  202.3 57.6 all-gather.7
  301.8 6.5 reduce-scatter.1
